TPU v7x, 32 devices: a whole 2x2x4 slice. The times are simulated.
32 devices in a mesh: ep: 8 (over z, x), tp: 4 (over y, core).
Axes of the slice: x: 2, y: 2, z: 4, core: 2. Of those that a mesh axis runs over, the one named last changes fastest.
Arguments:
- hidden_in: bfloat16 [128, 2048], P(None, 'ep'), may hold values from -24 to 24
- attn_gain: float32 [2048], replicated, may hold values from 0.1 to 1.9
- forget_weight: bfloat16 [2048, 16], replicated, may hold values from -0.125 to 0.125
- forget_bias: float32 [16], replicated, may hold values from -1 to 2
- query_weight: bfloat16 [2048, 2048], P('ep', 'tp'), may hold values from -0.125 to 0.125
- key_weight: bfloat16 [2048, 1024], P('ep', 'tp'), may hold values from -0.125 to 0.125
- value_weight: bfloat16 [2048, 1024], P('ep', 'tp'), may hold values from -0.125 to 0.125
- query_gain: float32 [128], replicated, may hold values from 0.1 to 1.9
- key_gain: float32 [128], replicated, may hold values from 0.1 to 1.9
- cache_keys: bfloat16 [128, 8, 1024, 128], P('ep', 'tp'), may hold values from -160 to 160
- cache_values: bfloat16 [128, 8, 1024, 128], P('ep', 'tp'), may hold values from -6 to 6
- cache_gates: float32 [128, 16, 1024], P('ep', 'tp'), may hold values from -256 to 0, as said below
- lengths: int32 [128], P('ep'), may hold values from 128 to 1024, as said below
- output_weight: bfloat16 [2048, 2048], P('tp', 'ep'), may hold values from -0.125 to 0.125
- ffn_gain: float32 [2048], replicated, may hold values from 0.1 to 1.9
- route_group: int32 [128], replicated, may hold values from 0 to 3, as said below
- route_expert: int32 [128, 2], replicated, may hold values from 0 to 3, as said below
- route_weight: float32 [128, 2], replicated, may hold values from 0.1 to 0.6
- expert_gate: bfloat16 [16, 2048, 1024], P('ep', None, 'tp'), may hold values from -0.125 to 0.125
- expert_up: bfloat16 [16, 2048, 1024], P('ep', None, 'tp'), may hold values from -0.125 to 0.125
- expert_down: bfloat16 [16, 1024, 2048], P('ep', 'tp'), may hold values from -0.1875 to 0.1875
- mix_vector: bfloat16 [2048], replicated, may hold values from -0.125 to 0.125
- dense_gate: bfloat16 [2048, 4096], P('ep', 'tp'), may hold values from -0.125 to 0.125
- dense_up: bfloat16 [2048, 4096], P('ep', 'tp'), may hold values from -0.125 to 0.125
- dense_down: bfloat16 [4096, 2048], P('tp', 'ep'), may hold values from -0.09375 to 0.09375
Outputs:
- mixed: bfloat16 [128, 2048], P(None, 'ep')
- fresh_keys: bfloat16 [128, 1024], P('ep', 'tp')
- fresh_values: bfloat16 [128, 1024], P('ep', 'tp')
Inputs may be any that keep to these rules, and one draw needn't show every extreme that they name: `cache_gates`: never rising along positions. `lengths`: some device holds a sequence of length 1024 in every draw. `route_group`: no expert is chosen by more than 24 tokens of the batch, and some expert by exactly 24. `route_expert`: a token's 2 experts differ; the loads of the experts of one group differ by at most two.
All inputs are finite; a program needn't handle non-finite values.
Results may differ from a plain program's by a relative error of at most 0.008.
Values may be sent and summed in bfloat16 or wider, within the bound.
A program may use at most 64 MiB of HBM per device.

v0:
```python
import jax
import jax.numpy as jnp
from jax import lax
from jax.sharding import PartitionSpec as P

D = 2048
HEAD_DIM = 128
GROUP_EXPERTS = 4
TOPK = 2
CAPACITY = 24


EPS = 1e-06


def head_norm(projected, gain_vec):
    return (
        projected
        * lax.rsqrt(jnp.mean(projected * projected, axis=-1, keepdims=True) + EPS)
        * gain_vec
    )


def slot_targets(route_group, route_expert, expert_count):
    chosen = (route_group[:, None] * GROUP_EXPERTS + route_expert).reshape(-1)
    onehot = (chosen[:, None] == jnp.arange(expert_count, dtype=jnp.int32)[None, :]).astype(
        jnp.int32
    )
    before = jnp.cumsum(onehot, axis=0) - onehot
    return chosen * CAPACITY + jnp.sum(before * onehot, axis=1)


def on_device(
    hidden_in,
    attn_gain,
    forget_weight,
    forget_bias,
    query_weight,
    key_weight,
    value_weight,
    query_gain,
    key_gain,
    cache_keys,
    cache_values,
    cache_gates,
    lengths,
    output_weight,
    ffn_gain,
    route_group,
    route_expert,
    route_weight,
    expert_gate,
    expert_up,
    expert_down,
    mix_vector,
    dense_gate,
    dense_up,
    dense_down,
):
    seq_count, width_block = hidden_in.shape
    own_count = cache_keys.shape[0]
    ep_index = lax.axis_index("ep")
    tp_index = lax.axis_index("tp")
    ep_count = lax.axis_size("ep")
    col_start = ep_index * width_block
    row_start = ep_index * own_count
    stream = hidden_in.astype(jnp.float32)
    normed_in = (stream * lax.dynamic_slice_in_dim(attn_gain, col_start, width_block)).astype(
        jnp.bfloat16
    )
    forget_rows = lax.dynamic_slice_in_dim(forget_weight, col_start, width_block, 0)
    squares, forget_dot = lax.psum(
        (
            jnp.sum(stream * stream, axis=1),
            jnp.dot(normed_in, forget_rows, preferred_element_type=jnp.float32),
        ),
        "ep",
    )
    inv_rms = lax.rsqrt(squares / D + EPS)
    query_cols = query_weight.shape[1]
    key_cols = key_weight.shape[1]
    selected = normed_in
    head_sums = lax.psum_scatter(
        jnp.concatenate(
            [
                jnp.dot(selected, query_weight, preferred_element_type=jnp.float32),
                jnp.dot(selected, key_weight, preferred_element_type=jnp.float32),
                jnp.dot(selected, value_weight, preferred_element_type=jnp.float32),
            ],
            axis=1,
        ),
        "ep",
        scatter_dimension=0,
        tiled=True,
    )
    heads_here = query_cols // HEAD_DIM
    kv_here = key_cols // HEAD_DIM
    group_size = heads_here // kv_here
    own_scale = lax.dynamic_slice_in_dim(inv_rms, row_start, own_count)
    query_rows = head_norm(
        head_sums[:, :query_cols].reshape(own_count, heads_here, HEAD_DIM), query_gain
    ).astype(jnp.bfloat16)
    fresh_key = head_norm(
        head_sums[:, query_cols : query_cols + key_cols].reshape(own_count, kv_here, HEAD_DIM),
        key_gain,
    ).astype(jnp.bfloat16)
    fresh_value = (head_sums[:, query_cols + key_cols :] * own_scale[:, None]).astype(jnp.bfloat16)
    gate_logit = lax.dynamic_slice(
        forget_dot, (row_start, tp_index * heads_here), (own_count, heads_here)
    )
    bias_here = lax.dynamic_slice_in_dim(forget_bias, tp_index * heads_here, heads_here)
    log_forget = jax.nn.log_sigmoid(gate_logit * own_scale[:, None] + bias_here)
    latest = jnp.take_along_axis(cache_gates, (lengths - 1)[:, None, None], axis=2)[:, :, 0]
    now_gate = (latest + log_forget).reshape(own_count, kv_here, group_size)
    grouped = query_rows.reshape(own_count, kv_here, group_size, HEAD_DIM)
    factor = HEAD_DIM ** (-0.5)
    scores = (
        jnp.einsum("skgd,skcd->skgc", grouped, cache_keys, preferred_element_type=jnp.float32)
        * factor
    )
    scores = scores + now_gate[..., None] - cache_gates.reshape(own_count, kv_here, group_size, -1)
    in_cache = (
        jnp.arange(cache_keys.shape[2], dtype=jnp.int32)[None, None, None, :]
        < lengths[:, None, None, None]
    )
    scores = jnp.where(in_cache, scores, -jnp.inf)
    self_score = (
        jnp.einsum("skgd,skd->skg", grouped, fresh_key, preferred_element_type=jnp.float32) * factor
    )
    ceiling = jnp.maximum(jnp.max(scores, axis=-1), self_score)
    weights = jnp.exp(scores - ceiling[..., None])
    self_weight = jnp.exp(self_score - ceiling)
    denominator = jnp.sum(weights, axis=-1) + self_weight
    mixed_heads = jnp.einsum(
        "skgc,skcd->skgd",
        weights.astype(jnp.bfloat16),
        cache_values,
        preferred_element_type=jnp.float32,
    )
    mixed_heads = mixed_heads + self_weight[..., None] * fresh_value.reshape(
        own_count, kv_here, 1, HEAD_DIM
    ).astype(jnp.float32)
    heads_out = (
        (mixed_heads / denominator[..., None]).reshape(own_count, query_cols).astype(jnp.bfloat16)
    )
    attn_part = jnp.dot(
        lax.all_gather(heads_out, "ep", axis=0, tiled=True),
        output_weight,
        preferred_element_type=jnp.float32,
    )
    attn_out = lax.psum(attn_part, "tp")
    middle = (stream + attn_out).astype(jnp.bfloat16).astype(jnp.float32)
    normed_mid = (middle * lax.dynamic_slice_in_dim(ffn_gain, col_start, width_block)).astype(
        jnp.bfloat16
    )
    mix_part = jnp.dot(
        normed_mid,
        lax.dynamic_slice_in_dim(mix_vector, col_start, width_block),
        preferred_element_type=jnp.float32,
    )
    squares_mid, mix_dot = lax.psum((jnp.sum(middle * middle, axis=1), mix_part), "ep")
    mid_scale = lax.rsqrt(squares_mid / D + EPS)
    mix_share = jax.nn.sigmoid(mid_scale * mix_dot)
    local_experts = expert_gate.shape[0]
    expert_count = local_experts * ep_count
    targets = slot_targets(route_group, route_expert, expert_count)
    slot_total = expert_count * CAPACITY
    slot_ids = jnp.arange(slot_total, dtype=jnp.int32)
    placed = jnp.any(
        targets.reshape(seq_count, TOPK)[None, :, :] == slot_ids[:, None, None], axis=2
    )
    outgoing = jnp.dot(placed.astype(jnp.bfloat16), normed_mid, preferred_element_type=jnp.float32)
    outgoing = outgoing.astype(jnp.bfloat16).reshape(ep_count, local_experts, CAPACITY, width_block)
    arrived = lax.all_to_all(outgoing, "ep", split_axis=0, concat_axis=3, tiled=True).reshape(
        local_experts, CAPACITY, -1
    )
    my_slots = lax.dynamic_slice_in_dim(
        placed, ep_index * local_experts * CAPACITY, local_experts * CAPACITY, 0
    )
    slot_scale = jnp.sum(jnp.where(my_slots, mid_scale[None, :], 0.0), axis=1).reshape(
        local_experts, CAPACITY, 1
    )
    gate_pre = (
        jnp.einsum("ecd,edf->ecf", arrived, expert_gate, preferred_element_type=jnp.float32)
        * slot_scale
    )
    up_pre = (
        jnp.einsum("ecd,edf->ecf", arrived, expert_up, preferred_element_type=jnp.float32)
        * slot_scale
    )
    expert_hidden = (jax.nn.silu(gate_pre) * up_pre).astype(jnp.bfloat16)
    expert_part = jnp.einsum(
        "ecf,efd->ecd", expert_hidden, expert_down, preferred_element_type=jnp.float32
    )
    returned = (
        lax.all_to_all(
            expert_part[None].astype(jnp.bfloat16), "ep", split_axis=3, concat_axis=0, tiled=True
        )
        .astype(jnp.float32)
        .reshape(slot_total, width_block)
    )
    picked = jnp.take(returned, targets, axis=0).reshape(seq_count, TOPK, width_block)
    routed = jnp.sum(picked * route_weight[:, :, None], axis=1)
    hidden_width = dense_gate.shape[1]
    selected = normed_mid
    both_sums = lax.psum_scatter(
        jnp.concatenate(
            [
                jnp.dot(selected, dense_gate, preferred_element_type=jnp.float32),
                jnp.dot(selected, dense_up, preferred_element_type=jnp.float32),
            ],
            axis=1,
        ),
        "ep",
        scatter_dimension=0,
        tiled=True,
    )
    gate_sum = both_sums[:, :hidden_width]
    up_sum = both_sums[:, hidden_width:]
    own_mid = lax.dynamic_slice_in_dim(mid_scale, row_start, own_count)
    dense_hidden = (jax.nn.silu(gate_sum * own_mid[:, None]) * (up_sum * own_mid[:, None])).astype(
        jnp.bfloat16
    )
    dense_part = jnp.dot(
        lax.all_gather(dense_hidden, "ep", axis=0, tiled=True),
        dense_down,
        preferred_element_type=jnp.float32,
    )
    ffn_total = lax.psum(
        (routed + mix_share[:, None] * dense_part).astype(jnp.bfloat16), "tp"
    ).astype(jnp.float32)
    mixed = (middle + ffn_total).astype(jnp.bfloat16)
    return (mixed, fresh_key.reshape(own_count, key_cols), fresh_value)


def solution(mesh):
    placed = (
        P(None, "ep"),
        P(),
        P(),
        P(),
        P("ep", "tp"),
        P("ep", "tp"),
        P("ep", "tp"),
        P(),
        P(),
        P("ep", "tp", None, None),
        P("ep", "tp", None, None),
        P("ep", "tp", None),
        P("ep"),
        P("tp", "ep"),
        P(),
        P(),
        P(),
        P(),
        P("ep", None, "tp"),
        P("ep", None, "tp"),
        P("ep", "tp", None),
        P(),
        P("ep", "tp"),
        P("ep", "tp"),
        P("tp", "ep"),
    )
    return jax.shard_map(
        on_device,
        mesh=mesh,
        in_specs=placed,
        out_specs=(P(None, "ep"), P("ep", "tp"), P("ep", "tp")),
        check_vma=False,
    )
```

profile of v0, /device:TPU:0, one launch (start us, length us, event | category | flops | bytes accessed | tf_op | source)
XLA Modules:
  0.0 295.3 jit_solution(9477003200772531910)
XLA Ops:
  7.3 0.9 dynamic_slice.27
  8.2 1.2 fusion.40
  9.4 1.1 fusion.36
  10.5 1.1 fusion.38
  11.6 0.9 pad_maximum_fusion.1
  12.7 0.8 fusion.34
  13.6 23.6 %all-reduce.1 = (f32[128,16]{0,1:T(8,128)S(1)}, f32[128]{0:T(128)S(1)}) all-reduce(f32[128,16]{0,1:T(8,128)S(1)} %fusion.34, f32[128]{0:T(128)S(1)} %fusion.15), channel_id=1, replica_groups=mesh['ep'=8,'tp'=4] {'ep'}, use_global_device_ids=true, to_apply=%region_2.0 | all-reduce | flops 2176 | bytes 17408 | tf_op jit(solution)/shard_map/psum | solution.py:72
  37.4 4.7 %copy.71 = f32[16,4,1024]{1,2,0:T(8,128)} copy(f32[16,4,1024]{2,1,0:T(4,128)S(1)} %copy-done.4) | data formatting | bytes 524288 | tf_op args[11]
  42.1 0.2 reshape.201
  42.3 0.1 copy.74
  42.4 0.1 eq.39
  42.5 0.7 reshape.203
  43.2 1.3 gather_fusion.1
  44.9 0.8 dynamic_slice.32
  45.7 0.8 dynamic_slice.34
  46.4 0.6 reshape.229
  47.0 0.6 reduce-window.6
  47.6 0.2 slice_reduce_fusion
  47.9 30.1 %reduce-scatter.3.cloned.1.call-done = f32[16,1024]{1,0:T(8,128)} async-done(((f32[128,1024]{1,0:T(8,128)}), f32[16,1024]{1,0:T(8,128)}) %reduce-scatter.3.cloned.1.call-update) | async-done | bytes 65552 | tf_op jit(solution)/shard_map/reduce_scatter | solution.py:83
  78.1 0.8 slice_multiply_fusion.3
  79.2 0.7 slice.33
  80.2 0.1 fusion.51
  80.4 5.8 %fusion.64 = (f32[16,2,2]{2,1,0:T(2,128)S(1)}, f32[16,2,2,1024]{3,2,1,0:T(2,128)S(1)}) fusion(f32[16,2,2,1024]{3,2,1,0:T(2,128)S(1)} %reshape.201, f32[16,2,2]{2,1,0:T(2,128)S(1)} %copy.73, bf16[16,2,2,128]{3,2,1,0:T(2,128)(2,1)S(1)} %multiply_convert_fusion, bf16[16,2,1024,128]{3,2,1,0:T(8,128)(2,1)} %param.34, pred[16,1024]{1,0:T(8,128)(4,1)S(1)} %iota_compare_fusion.1), kind=kOutput, calls=%fused_computation.109 | convolution fusion | flops 17104832 | bytes 8946176 | tf_op jit(solution)/shard_map/skgd,skcd->skgc/dot_general | solution.py:118
  86.2 0.3 fusion.11
  86.7 0.6 fusion.45
  87.3 5.4 %fusion.9 = bf16[16,2,2,128]{3,2,1,0:T(2,128)(2,1)} fusion(bf16[16,2,1024,128]{3,2,1,0:T(8,128)(2,1)} %param.35, f32[16,2,2,1024]{3,2,1,0:T(2,128)S(1)} %get-tuple-element.22, f32[16,2,2]{2,1,0:T(2,128)S(1)} %multiply_maximum_fusion, f32[16,2,2]{2,1,0:T(2,128)S(1)} %get-tuple-element.13, f32[16,2,128]{2,1,0:T(2,128)S(1)} %reshape.207, ...), kind=kOutput, calls=%fused_computation.18 | convolution fusion | flops 16941056 | bytes 8684288 | tf_op jit(solution)/shard_map/skgc,skcd->skgd/dot_general | solution.py:134
  92.7 0.8 convert_element_type.102
  93.5 30.5 %all_gather.6 = bf16[128,512]{1,0:T(8,128)(2,1)S(1)} all-gather(bf16[16,512]{1,0:T(8,128)(2,1)S(1)} %convert_element_type.102), channel_id=1, replica_groups=mesh['ep'=8,'tp'=4] {'ep'}, dimensions={0}, use_global_device_ids=true | all-gather | bytes 147456 | tf_op jit(solution)/shard_map/all_gather | solution.py:147
  124.0 0.8 fusion.65
  125.0 0.1 reduce_sum.81
  125.2 30.6 %all-reduce.5.cloned.1.call-done = f32[128,256]{1,0:T(8,128)} async-done(((f32[128,256]{1,0:T(8,128)}), f32[128,256]{1,0:T(8,128)}) %all-reduce.5.cloned.1.call-update) | async-done | bytes 131088 | tf_op jit(solution)/shard_map/psum | solution.py:151
  155.8 1.0 fusion.18
  156.9 0.2 fusion.28
  157.1 0.2 fusion.30
  157.3 1.1 pad_maximum_fusion
  158.5 0.9 convolution_convert_fusion.1
  159.4 5.5 %all-to-all-start = ((bf16[8,2,24,256]{3,2,1,0:T(8,128)(2,1)}), bf16[8,2,24,256]{3,2,1,0:T(8,128)(2,1)S(1)}, u32[]{:S(2)}, u32[]{:S(2)}) async-start(bf16[8,2,24,256]{3,2,1,0:T(8,128)(2,1)} %bitcast.9), calls=%async_computation.1 | async-start | bytes 393216 | tf_op jit(solution)/shard_map/all_to_all | solution.py:174
  164.9 0.1 convolution_bitcast_fusion
  165.0 21.9 %all-reduce = (f32[128]{0:T(128)S(1)}, f32[128]{0:T(128)S(1)}) all-reduce(f32[128]{0:T(128)S(1)} %get-tuple-element.11, f32[128]{0:T(128)S(1)} %convolution_bitcast_fusion), channel_id=1, replica_groups=mesh['ep'=8,'tp'=4] {'ep'}, use_global_device_ids=true, to_apply=%region_14.15 | all-reduce | flops 256 | bytes 2048 | tf_op jit(solution)/shard_map/psum | solution.py:161
  186.9 0.6 add_divide_fusion
  187.9 1.9 convolution_multiply_fusion.3
  189.9 2.3 fusion
  192.2 0.7 copy.80
  193.0 2.0 reshape.232
  195.0 3.4 %all-to-all-start.1 = ((bf16[8,2,6144]{2,1,0:T(2,128)(2,1)}), bf16[8,2,6144]{2,1,0:T(2,128)(2,1)S(1)}, u32[]{:S(2)}, u32[]{:S(2)}) async-start(bf16[8,2,6144]{2,1,0:T(2,128)(2,1)} %reshape.232), calls=%async_computation.2 | async-start | bytes 393216 | tf_op jit(solution)/shard_map/all_to_all | solution.py:196
  198.4 0.2 all-reduce.7.cloned.1.call-start
  198.6 0.1 copy.82
  198.7 0.1 mul.271
  198.9 0.1 copy.78
  199.0 0.7 copy.83
  199.8 0.6 pad_clamp_fusion
  200.4 0.6 dynamic_slice.35
  201.0 5.2 %all-to-all-done.1 = bf16[8,2,6144]{2,1,0:T(2,128)(2,1)S(1)} async-done(((bf16[8,2,6144]{2,1,0:T(2,128)(2,1)}), bf16[8,2,6144]{2,1,0:T(2,128)(2,1)S(1)}, u32[]{:S(2)}, u32[]{:S(2)}) %all-to-all-start.1) | async-done | bytes 196640 | tf_op jit(solution)/shard_map/all_to_all | solution.py:196
  206.1 1.5 reshape.233
  207.6 0.5 copy.81
  208.2 1.2 gather_fusion
  209.4 0.1 gather.15
  209.6 0.9 multiply_reduce_fusion
  210.5 13.5 %reduce-scatter.5.cloned.1.call-done = f32[16,2048]{1,0:T(8,128)} async-done(((f32[128,2048]{1,0:T(8,128)}), f32[16,2048]{1,0:T(8,128)}) %reduce-scatter.5.cloned.1.call-update) | async-done | bytes 131088 | tf_op jit(solution)/shard_map/reduce_scatter | solution.py:206
  224.0 1.0 fusion.22
  225.0 30.9 %all_gather.7 = bf16[128,1024]{1,0:T(8,128)(2,1)S(1)} all-gather(bf16[16,1024]{1,0:T(8,128)(2,1)S(1)} %fusion.22), channel_id=1, replica_groups=mesh['ep'=8,'tp'=4] {'ep'}, dimensions={0}, use_global_device_ids=true | all-gather | bytes 294912 | tf_op jit(solution)/shard_map/all_gather | solution.py:225
  255.8 0.9 fusion.5
  256.7 30.5 %all-reduce.7.cloned.1.call-done = bf16[128,256]{1,0:T(8,128)(2,1)} async-done(((bf16[128,256]{1,0:T(8,128)(2,1)}), bf16[128,256]{1,0:T(8,128)(2,1)}) %all-reduce.7.cloned.1.call-update) | async-done | bytes 65552 | tf_op jit(solution)/shard_map/psum | solution.py:229
  287.3 1.5 fusion.19
  (100 shorter events, 2.4 us)
Async XLA Ops:
  7.2 182.7 %copy-start = (bf16[2,256,2048]{2,1,0:T(8,128)(2,1)S(1)}, bf16[2,256,2048]{2,1,0:T(8,128)(2,1)}, u32[]{:S(2)}) copy-start(bf16[2,256,2048]{2,1,0:T(8,128)(2,1)} %param.45) | copy-start | bytes 6291460
  7.2 5.4 %copy-start.1 = (bf16[128,256]{1,0:T(8,128)(2,1)S(1)}, bf16[128,256]{1,0:T(8,128)(2,1)}, u32[]{:S(2)}) copy-start(bf16[128,256]{1,0:T(8,128)(2,1)} %param.25) | copy-start | bytes 196612
  7.2 5.5 %copy-start.20 = (s32[16]{0:T(128)S(1)}, s32[16]{0:T(128)}, u32[]{:S(2)}) copy-start(s32[16]{0:T(128)} %param.37) | copy-start | bytes 196
  7.2 6.4 %copy-start.21 = (s32[128]{0:T(128)S(1)}, s32[128]{0:T(128)}, u32[]{:S(2)}) copy-start(s32[128]{0:T(128)} %param.40) | copy-start | bytes 1540
  7.2 30.1 %copy-start.16 = (s32[128,2]{0,1:T(2,128)S(1)}, s32[128,2]{0,1:T(2,128)}, u32[]{:S(2)}) copy-start(s32[128,2]{0,1:T(2,128)} %param.41) | copy-start | bytes 3076
  7.2 30.1 %copy-start.4 = (f32[16,4,1024]{2,1,0:T(4,128)S(1)}, f32[16,4,1024]{2,1,0:T(4,128)}, u32[]{:S(2)}) copy-start(f32[16,4,1024]{2,1,0:T(4,128)} %param.36) | copy-start | bytes 786436
  7.2 70.8 %reduce-scatter.3.cloned.1.call-start = ((), (), s32[]{:S(2)}) async-start(), calls=%async_computation.4 | async-start | bytes 589824 | tf_op jit(solution)/shard_map/reduce_scatter | solution.py:83
  12.5 143.3 %all-reduce.5.cloned.1.call-start = ((), (), s32[]{:S(2)}) async-start(), calls=%async_computation.5 | async-start | bytes 262144 | tf_op jit(solution)/shard_map/psum | solution.py:151
  37.3 7.3 %copy-start.22 = (f32[16]{0:T(128)S(1)}, f32[16]{0:T(128)}, u32[]{:S(2)}) copy-start(f32[16]{0:T(128)} %param.28) | copy-start | bytes 196
  37.3 10.5 %copy-start.17 = (f32[128]{0:T(128)S(1)}, f32[128]{0:T(128)}, u32[]{:S(2)}) copy-start(f32[128]{0:T(128)} %param.33) | copy-start | bytes 1540
  37.4 42.7 %copy-start.18 = (f32[128]{0:T(128)S(1)}, f32[128]{0:T(128)}, u32[]{:S(2)}) copy-start(f32[128]{0:T(128)} %param.32) | copy-start | bytes 1540
  47.8 38.3 %copy-start.12 = (s32[16,3]{0,1:T(4,128)}, s32[16,3]{0,1:T(4,128)S(1)}, u32[]{:S(2)}) copy-start(s32[16,3]{0,1:T(4,128)S(1)} %reduce-window.9) | copy-start | bytes 580
  80.4 6.3 %copy-start.10 = (f32[16,1024]{1,0:T(8,128)S(1)}, f32[16,1024]{1,0:T(8,128)}, u32[]{:S(2)}) copy-start(f32[16,1024]{1,0:T(8,128)} %reduce-scatter.3.cloned.1.call-done) | copy-start | bytes 196612
  87.3 5.4 %copy-start.11 = (bf16[16,256]{1,0:T(8,128)(2,1)}, bf16[16,256]{1,0:T(8,128)(2,1)S(1)}, u32[]{:S(2)}) copy-start(bf16[16,256]{1,0:T(8,128)(2,1)S(1)} %get-tuple-element.16) | copy-start | bytes 24580
  87.3 36.7 %copy-start.8 = (bf16[512,256]{1,0:T(8,128)(2,1)S(1)}, bf16[512,256]{1,0:T(8,128)(2,1)}, u32[]{:S(2)}) copy-start(bf16[512,256]{1,0:T(8,128)(2,1)} %param.38) | copy-start | bytes 786436
  87.3 37.6 %slice-start = ((s32[16,3]{0,1:T(4,128)}), s32[16,2]{0,1:T(2,128)S(1)}, s32[]{:S(2)}) async-start(s32[16,3]{0,1:T(4,128)} %copy-done.12), calls=%async_computation.8 | async-start | bytes 2048 | tf_op jit(solution)/shard_map/slice.1
  87.3 37.6 %copy-start.13 = (s32[256]{0:T(256)S(1)}, s32[256]{0:T(256)}, u32[]{:S(2)}) copy-start(s32[256]{0:T(256)} %reshape.203) | copy-start | bytes 3076
  87.3 69.5 %copy-start.5 = (bf16[256,1024]{1,0:T(8,128)(2,1)S(1)}, bf16[256,1024]{1,0:T(8,128)(2,1)}, u32[]{:S(2)}) copy-start(bf16[256,1024]{1,0:T(8,128)(2,1)} %param.48) | copy-start | bytes 1572868
  92.7 64.4 %copy-start.6 = (bf16[256,1024]{1,0:T(8,128)(2,1)S(1)}, bf16[256,1024]{1,0:T(8,128)(2,1)}, u32[]{:S(2)}) copy-start(bf16[256,1024]{1,0:T(8,128)(2,1)} %param.47) | copy-start | bytes 1572868
  124.9 99.1 %reduce-scatter.5.cloned.1.call-start = ((), (), s32[]{:S(2)}) async-start(), calls=%async_computation.6 | async-start | bytes 1179648 | tf_op jit(solution)/shard_map/reduce_scatter | solution.py:206
  156.8 8.1 %copy-start.2 = (bf16[128,256]{1,0:T(8,128)(2,1)}, bf16[128,256]{1,0:T(8,128)(2,1)S(1)}, u32[]{:S(2)}) copy-start(bf16[128,256]{1,0:T(8,128)(2,1)S(1)} %get-tuple-element.12) | copy-start | bytes 196612
  157.3 7.6 %copy-start.23 = (bf16[256,1]{0,1:T(2,128)(2,1)S(1)}, bf16[256,1]{0,1:T(2,128)(2,1)}, u32[]{:S(2)}) copy-start(bf16[256,1]{0,1:T(2,128)(2,1)} %reshape.229) | copy-start | bytes 1540
  159.4 28.3 %all-to-all-start = ((bf16[8,2,24,256]{3,2,1,0:T(8,128)(2,1)}), bf16[8,2,24,256]{3,2,1,0:T(8,128)(2,1)S(1)}, u32[]{:S(2)}, u32[]{:S(2)}) async-start(bf16[8,2,24,256]{3,2,1,0:T(8,128)(2,1)} %bitcast.9), calls=%async_computation.1 | async-start | bytes 393216 | tf_op jit(solution)/shard_map/all_to_all | solution.py:174
  192.2 6.8 %copy-start.15 = (f32[128,2]{0,1:T(2,128)S(1)}, f32[128,2]{0,1:T(2,128)}, u32[]{:S(2)}) copy-start(f32[128,2]{0,1:T(2,128)} %param.42) | copy-start | bytes 3076
  195.0 11.1 %all-to-all-start.1 = ((bf16[8,2,6144]{2,1,0:T(2,128)(2,1)}), bf16[8,2,6144]{2,1,0:T(2,128)(2,1)S(1)}, u32[]{:S(2)}, u32[]{:S(2)}) async-start(bf16[8,2,6144]{2,1,0:T(2,128)(2,1)} %reshape.232), calls=%async_computation.2 | async-start | bytes 393216 | tf_op jit(solution)/shard_map/all_to_all | solution.py:196
  198.4 88.9 %all-reduce.7.cloned.1.call-start = ((), (), s32[]{:S(2)}) async-start(), calls=%async_computation.7 | async-start | bytes 131072 | tf_op jit(solution)/shard_map/psum | solution.py:229
  208.1 1.5 copy-start.9
  208.2 15.8 %copy-start.19 = (f32[16]{0:T(128)S(1)}, f32[16]{0:T(128)}, u32[]{:S(2)}) copy-start(f32[16]{0:T(128)} %dynamic_slice.35) | copy-start | bytes 196
  208.2 47.7 %copy-start.7 = (bf16[1024,256]{1,0:T(8,128)(2,1)S(1)}, bf16[1024,256]{1,0:T(8,128)(2,1)}, u32[]{:S(2)}) copy-start(bf16[1024,256]{1,0:T(8,128)(2,1)} %param.49) | copy-start | bytes 1572868
  208.2 47.7 %copy-start.14 = (f32[128]{0:T(128)S(1)}, f32[128]{0:T(128)}, u32[]{:S(2)}) copy-start(f32[128]{0:T(128)} %get-tuple-element.19) | copy-start | bytes 1540
  208.2 79.1 %copy-start.3 = (bf16[128,256]{1,0:T(8,128)(2,1)S(1)}, bf16[128,256]{1,0:T(8,128)(2,1)}, u32[]{:S(2)}) copy-start(bf16[128,256]{1,0:T(8,128)(2,1)} %copy-done.2) | copy-start | bytes 196612
Sparse Core Ops, SparseCore 0:
  12.6 65.3 reduce-scatter.2
  125.0 30.7 all-reduce.4
  159.2 64.7 reduce-scatter.4
  256.8 30.3 all-reduce.6
where the time goes:
time: 296 us; the launch traced here: 295 us
  waiting for transfers between devices  110 us (37%)
  blocking collectives  107 us (36%)
  matrix products  23 us (8%)
  local copies, waits for them, and re-layouts  21 us (7%)
  between operations  14.4 us (5%)
  other arithmetic  10.8 us (4%)
  starting transfers between devices  9.25 us (3%)
    all_gather x1, blocking collectives, on_device(): lax.all_gather(dense_hidden, 'ep', axis=0, tiled=True)  30.9 us
    psum x1, waiting for transfers between devices, on_device(): attn_out = lax.psum(attn_part, 'tp')  30.6 us
    psum x1, waiting for transfers between devices, on_device(): lax.psum((routed + mix_share[:, None] * dense_part).astype(jnp.bfloat16),...  30.5 us
    all_gather x1, blocking collectives, on_device(): lax.all_gather(heads_out, 'ep', axis=0, tiled=True)  30.5 us
    reduce_scatter x1, waiting for transfers between devices, on_device(): lax.psum_scatter(jnp.concatenate([jnp.dot(selected, query_weight, preferr...  30.1 us
    psum x1, blocking collectives, on_device(): lax.psum((jnp.sum(stream * stream, axis=1), jnp.dot(normed_in, forget_row...  23.6 us
    psum x1, blocking collectives, on_device(): lax.psum((jnp.sum(middle * middle, axis=1), mix_part), 'ep')  21.9 us
    reduce_scatter x1, waiting for transfers between devices, on_device(): lax.psum_scatter(jnp.concatenate([jnp.dot(selected, dense_gate, preferred...  13.5 us
  transfers between devices with their start and end apart: 6, of which 5 were waited for; matrix products, arithmetic and copies ran while one was open for 9% of the time, Pallas kernels for 0%

commit v1 on v0

v1 whole, which is shorter than its diff:
```python
import functools

import jax
import jax.numpy as jnp
from jax import lax
from jax.experimental import pallas as pl
from jax.experimental.pallas import tpu as pltpu
from jax.sharding import PartitionSpec as P

GROUP_EXPERTS = 4
TOPK = 2
CAPACITY = 24
EPS = 1e-06
MESH = pl.DeviceIdType.MESH
F32 = jnp.float32
BF16 = jnp.bfloat16


def mm(a, b):
    return jnp.dot(a, b, preferred_element_type=F32)


def mm_nt(a, b):
    return lax.dot_general(a, b, (((1,), (1,)), ((), ())), preferred_element_type=F32)


def layer_kernel(
    n,
    t,
    hidden,
    attn_gain,
    forget_bias,
    query_gain,
    key_gain,
    ffn_gain,
    mix_vector,
    route_group,
    route_expert,
    route_weight,
    lengths,
    fw_hbm,
    wq_hbm,
    wk_hbm,
    wv_hbm,
    ck_hbm,
    cv_hbm,
    gates_hbm,
    wo_hbm,
    eg_hbm,
    eu_hbm,
    ed_hbm,
    dg_hbm,
    du_hbm,
    dd_hbm,
    mixed_out,
    fk_out,
    fv_out,
    fw,
    wq,
    wk,
    wv,
    ck,
    cv,
    gates,
    wo,
    eg,
    eu,
    ed,
    dg,
    du,
    dd,
    q_rows,
    fk_rows,
    fv_rows,
    lf_rows,
    o_rows,
    mix_rows,
    placed_scr,
    placed_t,
    slot_rows,
    qkv_send,
    qkv_recv,
    st_send,
    st_recv,
    ag_buf,
    ar_buf,
    ms_buf,
    col_stats,
    dsp_send,
    dsp_recv,
    dn_send,
    dn_recv,
    ret_send,
    ret_recv,
    dh_buf,
    ar2_buf,
    w_sem,
    k_sem,
    v_sem,
    ep_send,
    ep_recv,
    tp_send,
    tp_recv,
):
    ep = lax.axis_index("ep")
    tp = lax.axis_index("tp")
    tokens, width = hidden.shape
    own = ck.shape[0]
    kv_here = ck.shape[1]
    positions = ck.shape[2]
    head_dim = ck.shape[3]
    q_cols = wq.shape[1]
    k_cols = wk.shape[1]
    heads = q_cols // head_dim
    group = heads // kv_here
    seqs = 8 // heads
    blocks = own // seqs
    model = n * width
    hidden_units = dg.shape[1]
    local_experts = eg.shape[0]
    slots_here = local_experts * CAPACITY
    slots = n * slots_here
    factor = head_dim ** (-0.5)

    plain = [
        (fw_hbm.at[:, pl.ds(pl.multiple_of(ep * width, width), width)], fw),
        (wq_hbm, wq),
        (wk_hbm, wk),
        (wv_hbm, wv),
        (gates_hbm, gates),
        (wo_hbm, wo),
        (dg_hbm, dg),
        (du_hbm, du),
        (eg_hbm, eg),
        (eu_hbm, eu),
        (ed_hbm, ed),
        (dd_hbm, dd),
    ]
    copies = [pltpu.make_async_copy(s, d, w_sem.at[i]) for i, (s, d) in enumerate(plain)]
    (c_fw, c_wq, c_wk, c_wv, c_gates, c_wo, c_dg, c_du, c_eg, c_eu, c_ed, c_dd) = copies

    def cache_copy(i, src, dst, sem):
        part = pl.ds(i * seqs, seqs)
        return pltpu.make_async_copy(src.at[part], dst.at[part], sem.at[i])

    for c in (c_fw, c_wq, c_wk, c_wv, c_gates):
        c.start()
    for i in range(blocks):
        cache_copy(i, ck_hbm, ck, k_sem).start()
        cache_copy(i, cv_hbm, cv, v_sem).start()
    for c in (c_wo, c_dg, c_du, c_eg, c_eu, c_ed, c_dd):
        c.start()

    barrier = pltpu.get_barrier_semaphore()
    for k in range(1, n):
        pl.semaphore_signal(
            barrier, inc=1, device_id={"ep": lax.rem(ep + k, n)}, device_id_type=MESH
        )
    for k in range(1, t):
        pl.semaphore_signal(
            barrier, inc=1, device_id={"tp": lax.rem(tp + k, t)}, device_id_type=MESH
        )

    def ep_copy(phase, peer, slot, src, dst):
        return pltpu.make_async_remote_copy(
            src_ref=src,
            dst_ref=dst,
            send_sem=ep_send.at[phase, peer],
            recv_sem=ep_recv.at[phase, slot],
            device_id={"ep": peer},
            device_id_type=MESH,
        )

    def tp_copy(phase, peer, slot, src, dst):
        return pltpu.make_async_remote_copy(
            src_ref=src,
            dst_ref=dst,
            send_sem=tp_send.at[phase, peer],
            recv_sem=tp_recv.at[phase, slot],
            device_id={"tp": peer},
            device_id_type=MESH,
        )

    ep_peers = [lax.rem(ep + k, n) for k in range(1, n)]
    tp_peers = [lax.rem(tp + k, t) for k in range(1, t)]

    def ep_start(phase, src_of, dst):
        for p in ep_peers:
            ep_copy(phase, p, ep, src_of(p), dst.at[ep]).start()

    def ep_wait(phase, src_of, dst):
        for p in ep_peers:
            ep_copy(phase, p, p, src_of(p), dst.at[p]).wait()

    def tp_start(phase, buf):
        for p in tp_peers:
            tp_copy(phase, p, tp, buf.at[tp], buf.at[tp]).start()

    def tp_wait(phase, buf):
        for p in tp_peers:
            tp_copy(phase, p, p, buf.at[tp], buf.at[p]).wait()

    def own_rows(ref):
        return lambda p: ref.at[pl.ds(pl.multiple_of(p * own, own), own), :]

    my_cols = pl.ds(pl.multiple_of(ep * width, width), width)

    stream = hidden[...].astype(F32)
    normed_in = (stream * attn_gain[:, my_cols]).astype(BF16)
    c_fw.wait()
    st_send[...] = jnp.broadcast_to(
        jnp.sum(stream * stream, axis=1, keepdims=True), st_send.shape
    )
    st_send[:, 0 : fw.shape[0]] = mm_nt(normed_in, fw[...])
    pl.semaphore_wait(barrier, n - 1 + t - 1)
    ep_start(0, own_rows(st_send), st_recv)
    c_wq.wait()
    qkv_send[:, 0:q_cols] = mm(normed_in, wq[...]).astype(BF16)
    c_wk.wait()
    qkv_send[:, q_cols : q_cols + k_cols] = mm(normed_in, wk[...]).astype(BF16)
    c_wv.wait()
    qkv_send[:, q_cols + k_cols :] = mm(normed_in, wv[...]).astype(BF16)
    ep_start(1, own_rows(qkv_send), qkv_recv)

    lane = lax.broadcasted_iota(jnp.int32, (tokens, 128), 1).astype(F32)
    sub_t = lax.broadcasted_iota(jnp.int32, (128, tokens), 0)
    chosen_rows = route_group[...].astype(F32) * GROUP_EXPERTS + route_expert[...].astype(F32)
    by_token = jnp.zeros((128, tokens), F32)
    for k in range(TOPK):
        by_token = jnp.where(sub_t == k, chosen_rows[k : k + 1, :], by_token)
    by_token = jnp.transpose(by_token, (1, 0))
    chosen = [by_token[:, k : k + 1] for k in range(TOPK)]
    onehot = [(lane == c).astype(F32) for c in chosen]
    earlier = (
        lax.broadcasted_iota(jnp.int32, (tokens, tokens), 1)
        < lax.broadcasted_iota(jnp.int32, (tokens, tokens), 0)
    ).astype(F32)
    before = mm(earlier.astype(BF16), sum(onehot).astype(BF16))
    target = [
        c * CAPACITY + jnp.sum(o * before, axis=1, keepdims=True) for c, o in zip(chosen, onehot)
    ]
    slot_lane = lax.broadcasted_iota(jnp.int32, (tokens, slots), 1).astype(F32)
    placed_t[...] = sum((slot_lane == g).astype(F32) for g in target).astype(BF16)
    packed = jnp.zeros((tokens, 128), F32)
    for k in range(TOPK):
        packed = jnp.where(lane == k, target[k], packed)
    rows = jnp.transpose(packed, (1, 0))[0:8, :]
    slot_rows[...] = rows
    slot_sub = lax.broadcasted_iota(jnp.int32, (slots, tokens), 0).astype(F32)
    placed_scr[...] = sum(
        (slot_sub == rows[k : k + 1, :]).astype(F32) for k in range(TOPK)
    ).astype(BF16)

    ep_wait(0, own_rows(st_send), st_recv)
    stats = st_send[pl.ds(pl.multiple_of(ep * own, own), own), :]
    for p in ep_peers:
        stats = stats + st_recv[p]
    own_scale = lax.rsqrt(stats[:, 127:128] / model + EPS)
    stat_lane = lax.broadcasted_iota(jnp.int32, stats.shape, 1)
    bias_lane = lax.broadcasted_iota(jnp.int32, forget_bias.shape, 1)
    ep_wait(1, own_rows(qkv_send), qkv_recv)
    sums = qkv_send[pl.ds(pl.multiple_of(ep * own, own), own), :].astype(F32)
    for p in ep_peers:
        sums = sums + qkv_recv[p].astype(F32)
    fresh_keys = []
    fresh_values = []
    for j in range(kv_here):
        at = q_cols + j * head_dim
        x = sums[:, at : at + head_dim]
        x = x * lax.rsqrt(jnp.mean(x * x, axis=1, keepdims=True) + EPS) * key_gain[...]
        x = x.astype(BF16)
        fk_out[:, j * head_dim : (j + 1) * head_dim] = x
        fresh_keys.append(x.astype(F32))
        at = q_cols + k_cols + j * head_dim
        y = (sums[:, at : at + head_dim] * own_scale).astype(BF16)
        fv_out[:, j * head_dim : (j + 1) * head_dim] = y
        fresh_values.append(y.astype(F32))
    for h in range(heads):
        x = sums[:, h * head_dim : (h + 1) * head_dim]
        x = x * lax.rsqrt(jnp.mean(x * x, axis=1, keepdims=True) + EPS) * query_gain[...]
        at = pl.ds(h, own, stride=heads)
        q_rows[at, :] = x.astype(BF16).astype(F32)
        fk_rows[at, :] = fresh_keys[h // group]
        fv_rows[at, :] = fresh_values[h // group]
        logit = jnp.sum(
            jnp.where(stat_lane == tp * heads + h, stats, 0.0), axis=1, keepdims=True
        )
        bias = jnp.sum(
            jnp.where(bias_lane == tp * heads + h, forget_bias[...], 0.0), axis=1, keepdims=True
        )
        z = logit * own_scale + bias
        log_forget = jnp.minimum(z, 0.0) - jnp.log1p(jnp.exp(-jnp.abs(z)))
        lf_rows[at, :] = jnp.broadcast_to(log_forget, (own, head_dim))

    c_gates.wait()
    row8 = lax.broadcasted_iota(jnp.int32, (8, positions), 0)
    pos8 = lax.broadcasted_iota(jnp.int32, (8, positions), 1)
    row_d = lax.broadcasted_iota(jnp.int32, (8, head_dim), 0)

    def attend(i, carry):
        at = pl.ds(pl.multiple_of(i * 8, 8), 8)
        q = q_rows[at, :]
        q16 = q.astype(BF16)
        self_score = jnp.sum(q * fk_rows[at, :], axis=1, keepdims=True) * factor
        limit = jnp.full((8, positions), 0, jnp.int32)
        for a in range(seqs):
            limit = jnp.where(row8 // heads == a, lengths[i * seqs + a], limit)
        g = jnp.concatenate([gates[i * seqs + a] for a in range(seqs)], axis=0)
        latest = jnp.sum(jnp.where(pos8 == limit - 1, g, 0.0), axis=1, keepdims=True)
        now = latest + lf_rows[at, 0:1]
        cache_copy(i, ck_hbm, ck, k_sem).wait()
        s = jnp.zeros((8, positions), F32)
        for a in range(seqs):
            for j in range(kv_here):
                one = mm_nt(q16, ck[i * seqs + a, j])
                s = jnp.where(row8 // group == a * kv_here + j, one, s)
        s = jnp.where(pos8 < limit, s * factor + now - g, -jnp.inf)
        ceiling = jnp.maximum(jnp.max(s, axis=1, keepdims=True), self_score)
        w = jnp.exp(s - ceiling)
        self_weight = jnp.exp(self_score - ceiling)
        denominator = jnp.sum(w, axis=1, keepdims=True) + self_weight
        w16 = w.astype(BF16)
        cache_copy(i, cv_hbm, cv, v_sem).wait()
        o = jnp.zeros((8, head_dim), F32)
        for a in range(seqs):
            for j in range(kv_here):
                one = mm(w16, cv[i * seqs + a, j])
                o = jnp.where(row_d // group == a * kv_here + j, one, o)
        o_rows[at, :] = (o + self_weight * fv_rows[at, :]) / denominator
        return carry

    lax.fori_loop(0, blocks, attend, 0)

    for h in range(heads):
        ag_buf[ep, :, h * head_dim : (h + 1) * head_dim] = o_rows[
            pl.ds(h, own, stride=heads), :
        ].astype(BF16)
    ep_start(2, lambda p: ag_buf.at[ep], ag_buf)
    c_wo.wait()
    ep_wait(2, lambda p: ag_buf.at[ep], ag_buf)
    ar_buf[tp] = mm(ag_buf[...].reshape(tokens, q_cols), wo[...]).astype(BF16)
    tp_start(0, ar_buf)
    tp_wait(0, ar_buf)
    attn_out = ar_buf[0].astype(F32)
    for p in range(1, t):
        attn_out = attn_out + ar_buf[p].astype(F32)
    middle = (hidden[...].astype(F32) + attn_out).astype(BF16)
    mixed_out[...] = middle
    middle = middle.astype(F32)
    normed_mid = (middle * ffn_gain[:, my_cols]).astype(BF16)

    sq = jnp.sum(middle * middle, axis=1, keepdims=True)
    mix_rows[...] = mix_vector[...].astype(F32)
    share_dot = jnp.zeros((tokens, 1), F32)
    for c in range(width // 128):
        mix_row = mix_rows[pl.ds(ep * (width // 128) + c, 1), :]
        share_dot += jnp.sum(
            normed_mid[:, c * 128 : (c + 1) * 128].astype(F32) * mix_row, axis=1, keepdims=True
        )
    both = jnp.where(lane < 4, sq, share_dot)
    ms_buf[ep] = jnp.transpose(both, (1, 0))[0:8, :]
    ep_start(3, lambda p: ms_buf.at[ep], ms_buf)
    dsp_send[...] = (
        mm(placed_scr[...], normed_mid).astype(BF16).reshape(n, slots_here, width)
    )
    dsp_recv[ep] = dsp_send[ep]
    ep_start(4, lambda p: dsp_send.at[p], dsp_recv)
    c_dg.wait()
    dn_send[:, 0:hidden_units] = mm(normed_mid, dg[...]).astype(BF16)
    c_du.wait()
    dn_send[:, hidden_units:] = mm(normed_mid, du[...]).astype(BF16)
    ep_start(5, own_rows(dn_send), dn_recv)

    ep_wait(3, lambda p: ms_buf.at[ep], ms_buf)
    total = ms_buf[0]
    for p in range(1, n):
        total = total + ms_buf[p]
    mid_row = lax.rsqrt(total[0:1, :] / model + EPS)
    share_row = jax.nn.sigmoid(mid_row * total[4:5, :])
    sub = lax.broadcasted_iota(jnp.int32, (128, tokens), 0)
    col_stats[...] = jnp.transpose(jnp.where(sub < 64, mid_row, share_row), (1, 0))
    slot_at = lax.broadcasted_iota(jnp.int32, (slots_here, tokens), 0) + ep * slots_here
    slot_at = slot_at.astype(F32)
    slot_scale = jnp.zeros((slots_here, 1), F32)
    slot_weight = jnp.zeros((slots_here, 1), F32)
    for k in range(TOPK):
        hit = slot_at == slot_rows[k : k + 1, :]
        slot_scale += jnp.sum(jnp.where(hit, mid_row, 0.0), axis=1, keepdims=True)
        slot_weight += jnp.sum(
            jnp.where(hit, route_weight[k : k + 1, :], 0.0), axis=1, keepdims=True
        )

    c_eg.wait()
    c_eu.wait()
    c_ed.wait()
    ep_wait(4, lambda p: dsp_send.at[p], dsp_recv)
    arrived = jnp.concatenate([dsp_recv[p] for p in range(n)], axis=1)

    def by_expert(results):
        row = lax.broadcasted_iota(jnp.int32, results[0].shape, 0)
        out = results[0]
        for e in range(1, local_experts):
            out = jnp.where(row >= e * CAPACITY, results[e], out)
        return out

    gate_pre = by_expert([mm(arrived, eg[e]) for e in range(local_experts)]) * slot_scale
    up_pre = by_expert([mm(arrived, eu[e]) for e in range(local_experts)]) * slot_scale
    expert_hidden = (jax.nn.silu(gate_pre) * up_pre).astype(BF16)
    for p in range(n):
        cols = slice(p * width, (p + 1) * width)
        part = by_expert([mm(expert_hidden, ed[e, :, cols]) for e in range(local_experts)])
        ret_send[p] = (part * slot_weight).astype(BF16)
    ret_recv[ep] = ret_send[ep]
    ep_start(6, lambda p: ret_send.at[p], ret_recv)

    ep_wait(5, own_rows(dn_send), dn_recv)
    my_rows = pl.ds(pl.multiple_of(ep * own, own), own)
    dense = dn_send[my_rows, :].astype(F32)
    for p in ep_peers:
        dense = dense + dn_recv[p].astype(F32)
    own_mid = col_stats[my_rows, 0:1]
    dh_buf[ep] = (
        jax.nn.silu(dense[:, 0:hidden_units] * own_mid) * (dense[:, hidden_units:] * own_mid)
    ).astype(BF16)
    ep_start(7, lambda p: dh_buf.at[ep], dh_buf)
    c_dd.wait()
    ep_wait(6, lambda p: ret_send.at[p], ret_recv)
    routed = mm(placed_t[...], ret_recv[...].reshape(slots, width))
    ep_wait(7, lambda p: dh_buf.at[ep], dh_buf)
    dense_part = mm(dh_buf[...].reshape(tokens, hidden_units), dd[...])
    ar2_buf[tp] = (routed + col_stats[:, 127:128] * dense_part).astype(BF16)
    tp_start(1, ar2_buf)
    tp_wait(1, ar2_buf)
    ffn = ar2_buf[0].astype(F32)
    for p in range(1, t):
        ffn = ffn + ar2_buf[p].astype(F32)
    mixed_out[...] = (mixed_out[...].astype(F32) + ffn).astype(BF16)


def hand_over(mixed, fresh_keys, fresh_values, mixed_out, fk_out, fv_out):
    mixed_out[...] = mixed[...]
    fk_out[...] = fresh_keys[...]
    fv_out[...] = fresh_values[...]


def on_device(
    hidden_in,
    attn_gain,
    forget_weight,
    forget_bias,
    query_weight,
    key_weight,
    value_weight,
    query_gain,
    key_gain,
    cache_keys,
    cache_values,
    cache_gates,
    lengths,
    output_weight,
    ffn_gain,
    route_group,
    route_expert,
    route_weight,
    expert_gate,
    expert_up,
    expert_down,
    mix_vector,
    dense_gate,
    dense_up,
    dense_down,
):
    n = lax.axis_size("ep")
    t = lax.axis_size("tp")
    tokens, width = hidden_in.shape
    own, kv_here, positions, head_dim = cache_keys.shape
    q_cols = query_weight.shape[1]
    k_cols = key_weight.shape[1]
    heads = q_cols // head_dim
    units = dense_gate.shape[1]
    slots_here = expert_gate.shape[0] * CAPACITY
    slots = n * slots_here
    rows = own * heads
    blocks = rows // 8

    def vm(shape, dtype):
        return pltpu.VMEM(shape, dtype)

    def like(x):
        return pltpu.VMEM(x.shape, x.dtype)

    big = [
        forget_weight.T,
        query_weight,
        key_weight,
        value_weight,
        cache_keys,
        cache_values,
        cache_gates,
        output_weight,
        expert_gate,
        expert_up,
        expert_down,
        dense_gate,
        dense_up,
        dense_down,
    ]
    small = [
        hidden_in,
        attn_gain[None],
        forget_bias[None],
        query_gain[None],
        key_gain[None],
        ffn_gain[None],
        mix_vector.reshape(-1, 128),
        route_group[None],
        route_expert.T,
        route_weight.T,
    ]
    vmem = pl.BlockSpec(memory_space=pltpu.VMEM)
    out_shape = (
        jax.ShapeDtypeStruct((tokens, width), BF16),
        jax.ShapeDtypeStruct((own, k_cols), BF16),
        jax.ShapeDtypeStruct((own, k_cols), BF16),
    )
    results = pl.pallas_call(
        functools.partial(layer_kernel, n, t),
        out_shape=out_shape,
        in_specs=[vmem] * len(small)
        + [pl.BlockSpec(memory_space=pltpu.SMEM)]
        + [pl.BlockSpec(memory_space=pl.ANY)] * len(big),
        out_specs=(vmem, vmem, vmem),
        scratch_shapes=[vm((forget_weight.shape[1], width), BF16)]
        + [like(x) for x in big[1:]]
        + [vm((rows, head_dim), F32)] * 5
        + [
            vm((n * width // 128, 128), F32),
            vm((slots, tokens), BF16),
            vm((tokens, slots), BF16),
            vm((8, tokens), F32),
            vm((tokens, q_cols + 2 * k_cols), BF16),
            vm((n, own, q_cols + 2 * k_cols), BF16),
            vm((tokens, 128), F32),
            vm((n, own, 128), F32),
            vm((n, own, q_cols), BF16),
            vm((t, tokens, width), BF16),
            vm((n, 8, tokens), F32),
            vm((tokens, 128), F32),
            vm((n, slots_here, width), BF16),
            vm((n, slots_here, width), BF16),
            vm((tokens, 2 * units), BF16),
            vm((n, own, 2 * units), BF16),
            vm((n, slots_here, width), BF16),
            vm((n, slots_here, width), BF16),
            vm((n, own, units), BF16),
            vm((t, tokens, width), BF16),
            pltpu.SemaphoreType.DMA((12,)),
            pltpu.SemaphoreType.DMA((blocks,)),
            pltpu.SemaphoreType.DMA((blocks,)),
            pltpu.SemaphoreType.DMA((8, n)),
            pltpu.SemaphoreType.DMA((8, n)),
            pltpu.SemaphoreType.DMA((2, t)),
            pltpu.SemaphoreType.DMA((2, t)),
        ],
        compiler_params=pltpu.CompilerParams(
            collective_id=0, has_side_effects=True, vmem_limit_bytes=58 * 1024 * 1024
        ),
    )(*small, lengths, *big)
    return pl.pallas_call(
        hand_over, out_shape=out_shape, in_specs=[vmem] * 3, out_specs=(vmem, vmem, vmem)
    )(*results)


def solution(mesh):
    placed = (
        P(None, "ep"),
        P(),
        P(),
        P(),
        P("ep", "tp"),
        P("ep", "tp"),
        P("ep", "tp"),
        P(),
        P(),
        P("ep", "tp", None, None),
        P("ep", "tp", None, None),
        P("ep", "tp", None),
        P("ep"),
        P("tp", "ep"),
        P(),
        P(),
        P(),
        P(),
        P("ep", None, "tp"),
        P("ep", None, "tp"),
        P("ep", "tp", None),
        P(),
        P("ep", "tp"),
        P("ep", "tp"),
        P("tp", "ep"),
    )
    return jax.shard_map(
        on_device,
        mesh=mesh,
        in_specs=placed,
        out_specs=(P(None, "ep"), P("ep", "tp"), P("ep", "tp")),
        check_vma=False,
    )
```

time: 296 us -> 68.8 us (0.23)
  waiting for transfers between devices: 110 us -> 0 us
  blocking collectives: 107 us -> 0 us
  Pallas kernels: 0 us -> 67.9 us
  matrix products: 23 us -> 0 us
  local copies, waits for them, and re-layouts: 21 us -> 0 us
  between operations: 14.4 us -> 0.65 us
  other arithmetic: 10.8 us -> 0 us
  starting transfers between devices: 9.25 us -> 0 us
    pallas_call x0 -> x2, Pallas kernels: none -> 67.9 us  [the longest x1 66.4 us: on_device(): pl.pallas_call(functools.partial(layer_kernel, n, t), out_shape=out_shape...]
    all_gather x2 -> x0, blocking collectives: 61.4 us -> none  [the longest x1 30.9 us: on_device(): lax.all_gather(dense_hidden, 'ep', axis=0, tiled=True)]
    psum x2 -> x0, waiting for transfers between devices: 61.1 us -> none  [the longest x1 30.6 us: on_device(): attn_out = lax.psum(attn_part, 'tp')]
    psum x2 -> x0, blocking collectives: 45.5 us -> none  [the longest x1 23.6 us: on_device(): lax.psum((jnp.sum(stream * stream, axis=1), jnp.dot(normed_in, forget_row...]
    reduce_scatter x2 -> x0, waiting for transfers between devices: 43.6 us -> none  [the longest x1 30.1 us: on_device(): lax.psum_scatter(jnp.concatenate([jnp.dot(selected, query_weight, preferr...]
    dot_general x15 -> x0, matrix products: 23 us -> none  [the longest x1 5.78 us: on_device(): jnp.einsum('skgd,skcd->skgc', grouped, cache_keys, preferred_element_type...]
    unnamed x54 -> x0, local copies, waits for them, and re-layouts: 9.15 us -> none
    all_to_all x2 -> x0, starting transfers between devices: 8.9 us -> none  [the longest x1 5.51 us: on_device(): lax.all_to_all(outgoing, 'ep', split_axis=0, concat_axis=3, tiled=True)]
  transfers between devices with their start and end apart: 6 -> 0, of which waited for: 5 -> 0; matrix products, arithmetic and copies ran while one was open for 9% -> 0% of each run, Pallas kernels for 0% -> 0%
where the time goes in v1:
time: 68.8 us; the launch traced here: 68.5 us
  Pallas kernels  67.9 us (99%)
    pallas_call x1, Pallas kernels, on_device(): pl.pallas_call(functools.partial(layer_kernel, n, t), out_shape=out_shape...  66.4 us
    pallas_call x1, Pallas kernels, on_device(): pl.pallas_call(hand_over, out_shape=out_shape, in_specs=[vmem] * 3, out_s...  1.5 us

profile of v1, /device:TPU:0, one launch (start us, length us, event | category | flops | bytes accessed | tf_op | source)
XLA Modules:
  0.0 68.5 jit_solution(1716698023880057101)
XLA Ops:
  0.6 66.4 %shard_map.256 = (bf16[128,256]{1,0:T(8,128)(2,1)}, bf16[16,256]{1,0:T(8,128)(2,1)}, bf16[16,256]{1,0:T(8,128)(2,1)}) custom-call(bf16[128,256]{1,0:T(8,128)(2,1)} %hidden.1, f32[1,2048]{1,0:T(1,128)} %bitcast.11, f32[1,16]{1,0:T(1,128)} %bitcast.16, f32[1,128]{1,0:T(1,128)} %bitcast.17, f32[1,128]{1,0:T(1,128)} %bitcast.18, f32[1,2048]{1,0:T(1,128)} %bitcast.12, ...), custom_call_target="tpu_custom_call" | custom-call | tf_op jit(solution)/shard_map/pallas_call | solution.py:526
  67.0 1.5 %shard_map.257 = (bf16[128,256]{1,0:T(8,128)(2,1)}, bf16[16,256]{1,0:T(8,128)(2,1)}, bf16[16,256]{1,0:T(8,128)(2,1)}) custom-call(bf16[128,256]{1,0:T(8,128)(2,1)} %get-tuple-element.6.mixed, bf16[16,256]{1,0:T(8,128)(2,1)} %get-tuple-element.7.fresh_keys, bf16[16,256]{1,0:T(8,128)(2,1)} %get-tuple-element.8.fresh_values), custom_call_target="tpu_custom_call" | custom-call | tf_op jit(solution)/shard_map/pallas_call | solution.py:569
